TPU v7x, 32 devices: a whole 2x2x4 slice. The times are simulated.
32 devices in a mesh: sp: 16 (over z, y, x), tp: 2 (over core).
Axes of the slice: x: 2, y: 2, z: 4, core: 2. Of those that a mesh axis runs over, the one named last changes fastest.
Arguments:
- inputs: bfloat16 [4096, 2048], P('sp', 'tp'), may hold values from -200 to 200
- input_gain: bfloat16 [2048], P('tp'), may hold values from 0.099609375 to 1.8984375
- stick_query_w: bfloat16 [2048, 1024], P(None, 'tp'), may hold values from -0.3125 to 0.3125
- stick_key_w: bfloat16 [2048, 1024], P(None, 'tp'), may hold values from -0.125 to 0.125
- stick_value_w: bfloat16 [2048, 1024], P(None, 'tp'), may hold values from -0.125 to 0.125
- ret_query_w: bfloat16 [2048, 2048], P(None, 'tp'), may hold values from -0.125 to 0.125
- ret_key_w: bfloat16 [2048, 2048], P(None, 'tp'), may hold values from -0.125 to 0.125
- ret_value_w: bfloat16 [2048, 2048], P(None, 'tp'), may hold values from -0.125 to 0.125
- stick_offset: float32 [8], P('tp'), may hold values from -17 to -2
- ret_log_decay: float32 [8], P('tp'), may hold values from -0.04 to 0, as said below
- initial_state: float32 [8, 256, 256], P('tp', 'sp'), may hold values from -38.4 to 38.4
- stick_gain: float32 [1024], P('tp'), may hold values from 0.1 to 1.9
- ret_gain: float32 [2048], P('tp'), may hold values from 0.1 to 1.9
- stick_out_w: bfloat16 [1024, 2048], P('tp', 'sp'), may hold values from -0.125 to 0.125
- ret_out_w: bfloat16 [2048, 2048], P('tp', 'sp'), may hold values from -0.09375 to 0.09375
Outputs:
- layer_out: bfloat16 [4096, 2048], P(('sp', 'tp'))
Inputs may be any that keep to these rules, and one draw needn't show every extreme that they name: `ret_log_decay`: every entry is negative.
All inputs are finite; a program needn't handle non-finite values.
Results may differ from a plain program's by a relative error of at most 0.017.
Values may be sent and summed in bfloat16 or wider, within the bound.
A program may use at most 128 MiB of HBM per device.

v0:
```python
import jax
import jax.numpy as jnp
from jax import lax
from jax.sharding import PartitionSpec as P

D = 2048
STICK_HEADS = 8
STICK_DIM = 128
epsilon = 1e-06
rope_base = 10000.0


def entering_2(value, axis, join, neutral):
    count, mine = (lax.axis_size(axis), lax.axis_index(axis))
    pieces = jax.tree.map(lambda part: lax.all_gather(part, axis), value)
    running = jax.tree.map(
        lambda part, zero: jnp.full_like(part, 0) + jnp.asarray(zero, part.dtype), value, neutral
    )

    def hop(position, running):
        longer = join(running, jax.tree.map(lambda part: part[position], pieces))
        return jax.tree.map(lambda new, old: jnp.where(position < mine, new, old), longer, running)

    return lax.fori_loop(0, count - 1, hop, running)


def rotate(values, positions):
    half_width = values.shape[-1] // 2
    inverse = rope_base ** (-jnp.arange(half_width, dtype=jnp.float32) / half_width)
    angles = positions.astype(jnp.float32)[:, None] * inverse[None, :]
    cosine = jnp.cos(angles)[:, None, :]
    sine_table = jnp.sin(angles)[:, None, :]
    first_half = values[..., :half_width]
    second_half = values[..., half_width:]
    return jnp.concatenate(
        [
            first_half * cosine - second_half * sine_table,
            second_half * cosine + first_half * sine_table,
        ],
        axis=-1,
    )


def stick_block(partial_state, queries, key_rows, value_rows, offsets, query_pos, key_pos):
    running, before = partial_state
    score_scale = queries.shape[2] ** (-0.5)
    scores = (
        jnp.einsum("thd,shd->hts", queries, key_rows, preferred_element_type=jnp.float32)
        * score_scale
        + offsets[:, None, None]
    )
    allowed = ((key_pos[None, :] < query_pos[:, None]) & (key_pos[None, :] >= 0))[None]
    remain = jnp.where(allowed, jax.nn.log_sigmoid(-scores), 0.0)
    suffix = lax.cumsum(remain, axis=2, reverse=True) - remain + before[:, :, None]
    weights = jnp.where(allowed, jnp.exp(jax.nn.log_sigmoid(scores) + suffix), 0.0).astype(
        jnp.bfloat16
    )
    running = running + jnp.einsum(
        "hts,shd->thd", weights, value_rows, preferred_element_type=jnp.float32
    )
    return (running, before + jnp.sum(remain, axis=2))


def sweep_keys(keys_all, values_all, query_rows, positions, offsets, key_span):
    row_count, head_count, head_width = query_rows.shape
    span_offsets = jnp.arange(key_span, dtype=jnp.int32)
    needed = (positions[row_count - 1] + key_span) // key_span

    def visit(visit_index, partial_state):
        key_start = (needed - 1 - visit_index) * key_span
        key_rows = lax.dynamic_slice_in_dim(keys_all, key_start, key_span, 0).reshape(
            key_span, head_count, head_width
        )
        value_rows = lax.dynamic_slice_in_dim(values_all, key_start, key_span, 0).reshape(
            key_span, head_count, head_width
        )
        return stick_block(
            partial_state,
            query_rows,
            key_rows,
            value_rows,
            offsets,
            positions,
            key_start + span_offsets,
        )

    start_carry = (
        jnp.zeros((row_count, head_count, head_width), jnp.float32),
        jnp.zeros((head_count, row_count), jnp.float32),
    )
    final_state = lax.fori_loop(0, needed, visit, start_carry)
    return final_state[0]


def body(
    inputs,
    input_gain,
    stick_query_w,
    stick_key_w,
    stick_value_w,
    ret_query_w,
    ret_key_w,
    ret_value_w,
    stick_offset,
    ret_log_decay,
    initial_state,
    stick_gain,
    ret_gain,
    stick_out_w,
    ret_out_w,
):
    tok_rows = inputs.shape[0]
    matrices = (stick_query_w, stick_key_w, stick_value_w, ret_query_w, ret_key_w, ret_value_w)
    own_squares = jnp.sum(jnp.square(inputs.astype(jnp.float32)), axis=1)
    squares = lax.psum(own_squares, "tp")
    scaled = (
        lax.all_gather(inputs, "tp", axis=1, tiled=True).astype(jnp.float32)
        * lax.all_gather(input_gain[None, :], "tp", axis=1, tiled=True).astype(jnp.float32)
    ).astype(jnp.bfloat16)
    projected = tuple(
        (jnp.dot(scaled, matrix, preferred_element_type=jnp.float32) for matrix in matrices)
    )
    row_scale = lax.rsqrt(squares / D + epsilon)
    stick_query, stick_key, stick_value, ret_query, ret_key, ret_value = tuple(
        ((running * row_scale[:, None]).astype(jnp.bfloat16) for running in projected)
    )
    head_count = stick_offset.shape[0]
    head_width = stick_query.shape[1] // head_count
    first_pos = lax.axis_index("sp") * tok_rows
    query_pos = first_pos + jnp.arange(tok_rows, dtype=jnp.int32)
    queries = stick_query.reshape(tok_rows, head_count, head_width)
    key_span = 4 * tok_rows
    keys_all, values_all = (
        lax.all_gather(stick_key, "sp", axis=0, tiled=True),
        lax.all_gather(stick_value, "sp", axis=0, tiled=True),
    )
    stick_total = sweep_keys(keys_all, values_all, queries, query_pos, stick_offset, key_span)
    stick_local = jnp.sum(jnp.square(stick_total), axis=(1, 2))
    stick_squares = lax.psum(stick_local, "tp")
    stick_scale = lax.rsqrt(stick_squares / (STICK_HEADS * STICK_DIM) + epsilon)
    stick_normed = (
        stick_total.reshape(tok_rows, head_count * head_width) * stick_scale[:, None] * stick_gain
    ).astype(jnp.bfloat16)
    state_full = lax.all_gather(initial_state, "sp", axis=1, tiled=True)
    ret_heads = ret_log_decay.shape[0]
    ret_width = ret_query.shape[1] // ret_heads
    turned_query = rotate(
        ret_query.reshape(tok_rows, ret_heads, ret_width).astype(jnp.float32), query_pos
    )
    turned_key = rotate(
        ret_key.reshape(tok_rows, ret_heads, ret_width).astype(jnp.float32), query_pos
    ) * ret_width ** (-0.5)
    ret_values = ret_value.reshape(tok_rows, ret_heads, ret_width).astype(jnp.float32)
    local_pos = jnp.arange(tok_rows, dtype=jnp.float32)
    distance = local_pos[:, None] - local_pos[None, :]
    decay_mask = jnp.where(
        distance[None] >= 0.0,
        jnp.exp(ret_log_decay[:, None, None] * jnp.maximum(distance, 0.0)[None]),
        0.0,
    )
    highest = lax.Precision.HIGHEST
    scores = jnp.einsum("thd,shd->hts", turned_query, turned_key, precision=highest) * decay_mask
    inner_part = jnp.einsum("hts,she->the", scores, ret_values, precision=highest)
    key_decay = jnp.exp(ret_log_decay[None, :] * (tok_rows - 1.0 - local_pos[:, None]))
    own_state = jnp.einsum(
        "shd,she->hde", turned_key * key_decay[:, :, None], ret_values, precision=highest
    )
    block_decay = jnp.exp(ret_log_decay * tok_rows)

    def join_states(earlier, later):
        return (earlier[0] * later[1][:, None, None] + later[0], earlier[1] * later[1])

    prefix_state, _ = entering_2(
        (own_state, block_decay),
        "sp",
        join_states,
        (jnp.zeros_like(own_state), jnp.ones_like(block_decay)),
    )
    entering = (
        prefix_state
        + jnp.exp(ret_log_decay * first_pos.astype(jnp.float32))[:, None, None] * state_full
    )
    query_decay = jnp.exp(ret_log_decay[None, :] * (local_pos[:, None] + 1.0))
    cross_part = (
        jnp.einsum("thd,hde->the", turned_query, entering, precision=highest)
        * query_decay[:, :, None]
    )
    ret_total = inner_part + cross_part
    centered = ret_total - jnp.mean(ret_total, axis=2, keepdims=True)
    normed = centered * lax.rsqrt(jnp.mean(centered * centered, axis=2, keepdims=True) + epsilon)
    ret_normed = (normed.reshape(tok_rows, ret_heads * ret_width) * ret_gain).astype(jnp.bfloat16)
    stick_cols, ret_cols = (
        lax.all_gather(stick_out_w, "sp", axis=1, tiled=True),
        lax.all_gather(ret_out_w, "sp", axis=1, tiled=True),
    )
    stick_part = jnp.dot(stick_normed, stick_cols, preferred_element_type=jnp.float32)
    return lax.psum_scatter(
        (stick_part + jnp.dot(ret_normed, ret_cols, preferred_element_type=jnp.float32)).astype(
            jnp.bfloat16
        ),
        "tp",
        scatter_dimension=0,
        tiled=True,
    )


def solution(mesh):
    in_specs = (
        P("sp", "tp"),
        P("tp"),
        P(None, "tp"),
        P(None, "tp"),
        P(None, "tp"),
        P(None, "tp"),
        P(None, "tp"),
        P(None, "tp"),
        P("tp"),
        P("tp"),
        P("tp", "sp", None),
        P("tp"),
        P("tp"),
        P("tp", "sp"),
        P("tp", "sp"),
    )
    out_specs = P(("sp", "tp"), None)
    return jax.shard_map(body, mesh=mesh, in_specs=in_specs, out_specs=out_specs, check_vma=False)
```

profile of v0, /device:TPU:0, one launch (start us, length us, event | category | flops | bytes accessed | tf_op | source)
XLA Modules:
  0.0 597.4 jit_solution(9106212903124527146)
XLA Ops:
  6.5 0.7 all-gather.11.cloned.1.call-update
  7.3 2.1 all-gather
  9.4 1.2 multiply_reduce_fusion.1
  10.7 2.5 psum.14
  13.1 7.5 %all-gather.11.cloned.1.call-done = bf16[256,2048]{1,0:T(8,128)(2,1)} async-done(((bf16[256,1024]{1,0:T(8,128)(2,1)}), bf16[256,2048]{1,0:T(8,128)(2,1)}) %all-gather.11.cloned.1.call-update) | async-done | bytes 1048592 | tf_op jit(solution)/shard_map/all_gather | solution.py:117
  20.7 2.7 fusion.29
  23.5 3.0 fusion.30
  26.7 0.5 multiply_cosine_fusion
  27.3 3.4 fusion.26
  31.2 4.0 fusion.28
  36.4 1.5 copy-done.15
  38.2 1.3 fusion.24
  39.5 2.2 fusion.36
  41.7 0.5 all-gather.19.cloned.1.call-update
  42.9 0.7 all-gather.17.cloned.1.call-update
  43.8 0.6 slice.25
  45.0 0.6 dynamic-slice
  46.4 43.1 %all-reduce = f32[64]{0:T(128)S(1)} all-reduce(f32[64]{0:T(128)S(1)} %get-tuple-element.346), channel_id=3, replica_groups=mesh['sp'=16,'tp'=2] {'sp'}, use_global_device_ids=true, to_apply=%add | all-reduce | flops 64 | bytes 512
  89.6 1.3 convolution_multiply_fusion
  90.9 1.8 convolution_bitcast_fusion.2
  92.7 0.7 fusion.32
  93.4 0.8 copy.90
  94.2 6.5 %all-gather.13.cloned.1.call-done = bf16[4096,512]{1,0:T(8,128)(2,1)} async-done(((bf16[256,512]{1,0:T(8,128)(2,1)}), bf16[4096,512]{1,0:T(8,128)(2,1)}) %all-gather.13.cloned.1.call-update) | async-done | bytes 4194320 | tf_op jit(solution)/shard_map/all_gather | solution.py:135
  100.7 77.1 %all-gather.15.cloned.1.call-done = bf16[4096,512]{1,0:T(8,128)(2,1)} async-done(((bf16[256,512]{1,0:T(8,128)(2,1)}), bf16[4096,512]{1,0:T(8,128)(2,1)}) %all-gather.15.cloned.1.call-update) | async-done | bytes 4194320 | tf_op jit(solution)/shard_map/all_gather | solution.py:134
  177.8 0.9 broadcast_in_dim.37
  178.7 34.5 %while.29 = (s32[]{:T(128)}, f32[256,4,128]{0,2,1:T(8,128)}, f32[4,256]{1,0:T(4,128)S(1)}, s32[]{:T(128)}, s32[]{:T(128)}, /*index=5*/bf16[4096,512]{1,0:T(8,128...) while((s32[]{:T(128)}, f32[256,4,128]{0,2,1:T(8,128)}, ...), condition=%wide.region_6.7_spmd.clone, body=%wide.region_2.6_spmd.clone.sunk | while | flops 707463424 | bytes 96735608 | solution.py:91
  178.7 1.7 constant_dynamic-slice_fusion.3
  180.4 0.5 copy.96
  181.3 0.5 copy.97
  181.8 6.3 %fusion.89 = (f32[4,256]{1,0:T(4,128)S(1)}, f32[4,256,1024]{1,2,0:T(8,128)S(1)}, f32[4,1024,256]{2,1,0:T(8,128)}) fusion(f32[4]{0:T(128)S(1)} %get-tuple-element.519, pred[256,1024]{0,1:T(8,128)(4,1)S(1)} %compare_and_fusion.2, bf16[1024,4,128]{0,2,1:T(8,128)(2,1)S(1)} %bitcast.121, bf16[256,4,128]{2,0,1:T(8,128)(2,1)} %get-tuple-element.518), kind=kOutput, calls=%fused_computation.33.clone.1 | convolution fusion | flops 279968768 | bytes 9965584 | tf_op jit(solution)/shard_map/while/body/thd,shd->hts/dot_general | solution.py:48
  188.1 10.1 %fusion.90 = f32[4,256,8,128]{1,2,3,0:T(8,128)S(1)} fusion(f32[4,256,8,128]{1,3,2,0:T(8,128)S(1)} %bitcast.119), kind=kOutput, calls=%fused_computation.20.clone.1 | output fusion | flops 133169152 | bytes 8388608 | tf_op jit(solution)/shard_map/reduce-window.4
  198.2 2.1 copy-done.2
  200.3 2.7 broadcast_add_fusion.2
  203.0 1.3 copy.98
  204.3 0.9 copy-done.3
  205.2 6.6 %fusion.91 = bf16[4,256,1024]{1,2,0:T(8,128)(2,1)S(1)} fusion(f32[4,256,8,128]{1,3,2,0:T(8,128)S(1)} %copy.98, f32[4,1024,256]{2,1,0:T(8,128)S(1)} %copy-done.3, f32[4,256]{1,0:T(4,128)S(1)} %get-tuple-element.498, f32[4]{0:T(128)S(1)} %get-tuple-element.519, pred[256,1024]{0,1:T(8,128)(4,1)S(1)} %compare_and_fusion.2), kind=kLoop, calls=%fused_computation.8.clone.1 | loop fusion | flops 24117248 | bytes 10752016 | tf_op jit(solution)/shard_map/while/body/convert_element_type | solution.py:55
  212.4 0.8 copy-done.5
  213.2 1.1 multiply_reduce_fusion.2
  214.3 2.7 psum.15
  217.0 1.2 fusion.42
  218.2 151.9 %all-gather.23.cloned.1.call-done = f32[64,256,256]{2,1,0:T(8,128)} async-done(((f32[4,256,256]{2,1,0:T(8,128)}), f32[64,256,256]{2,1,0:T(8,128)}) %all-gather.23.cloned.1.call-update) | async-done | bytes 16777232 | tf_op jit(solution)/shard_map/all_gather | solution.py:15
  370.1 41.3 %while.30 = (s32[]{:T(128)}, f32[4,256,256]{2,1,0:T(8,128)}, s32[]{:T(128)}, f32[16,4]{1,0:T(8,128)S(1)}, f32[16,4,256,256]{3,2,1,0:T(8,128)}, /*index=5*/s32[]{:T(128)}, s32[]{:T(128)}) while((s32[]{:T(128)}, f32[4,256,256]{2,1,0:T(8,128)}, s32[]{:T(128)}, f32[16,4]{1,0:T(8,128)S(1)}, f32[16,4,256,256]{3,2,1,0:T(8,128)}, ...), condition=%wide.region_10.11_spmd.clone, body=%wide.region_9.10_spmd.clone.sunk | while | flops 1048580 | bytes 3145889 | solution.py:24
  370.1 2.6 fusion.93
  372.7 2.7 fusion.93
  375.4 2.7 fusion.93
  378.2 2.8 fusion.93
  381.0 2.7 fusion.93
  383.7 2.8 fusion.93
  386.5 2.7 fusion.93
  389.2 2.7 fusion.93
  392.0 2.7 fusion.93
  394.7 2.8 fusion.93
  397.6 2.7 fusion.93
  400.3 2.7 fusion.93
  403.1 2.8 fusion.93
  405.8 2.7 fusion.93
  408.6 2.7 fusion.93
  411.3 14.5 %all-gather.19.cloned.1.call-done = f32[4,256,256]{2,1,0:T(8,128)} async-done(((f32[4,16,256]{2,1,0:T(8,128)}), f32[4,256,256]{2,1,0:T(8,128)}) %all-gather.19.cloned.1.call-update) | async-done | bytes 1048592 | tf_op jit(solution)/shard_map/all_gather | solution.py:144
  425.8 3.5 fusion.57
  429.8 86.2 %all-gather.21.cloned.1.call-done = bf16[1024,2048]{1,0:T(8,128)(2,1)} async-done(((bf16[1024,128]{1,0:T(8,128)(2,1)}), bf16[1024,2048]{1,0:T(8,128)(2,1)}) %all-gather.21.cloned.1.call-update) | async-done | bytes 4194320 | tf_op jit(solution)/shard_map/all_gather | solution.py:194
  516.0 4.9 fusion.58
  520.9 58.9 %all-gather.17.cloned.1.call-done = bf16[512,2048]{1,0:T(8,128)(2,1)} async-done(((bf16[512,128]{1,0:T(8,128)(2,1)}), bf16[512,2048]{1,0:T(8,128)(2,1)}) %all-gather.17.cloned.1.call-update) | async-done | bytes 2097168 | tf_op jit(solution)/shard_map/all_gather | solution.py:193
  579.8 3.9 fusion.21
  583.8 6.7 %reduce-scatter.2.cloned.1.call-done = bf16[128,2048]{1,0:T(8,128)(2,1)} async-done(((bf16[256,2048]{1,0:T(8,128)(2,1)}), bf16[128,2048]{1,0:T(8,128)(2,1)}) %reduce-scatter.2.cloned.1.call-update) | async-done | bytes 524304 | tf_op jit(solution)/shard_map/reduce_scatter | solution.py:197
  (98 shorter events, 4.8 us)
Async XLA Ops:
  6.5 14.1 %copy-start = (bf16[2048,512]{1,0:T(8,128)(2,1)S(1)}, bf16[2048,512]{1,0:T(8,128)(2,1)}, u32[]{:S(2)}) copy-start(bf16[2048,512]{1,0:T(8,128)(2,1)} %param.23) | copy-start | bytes 6291460
  6.5 14.1 %all-gather.11.cloned.1.call-start = ((), (), s32[]{:S(2)}) async-start(), calls=%async_computation.1 | async-start | bytes 1572864 | tf_op jit(solution)/shard_map/all_gather | solution.py:117
  7.3 93.4 %all-gather.13.cloned.1.call-start = ((), (), s32[]{:S(2)}) async-start(), calls=%async_computation.2 | async-start | bytes 4456448 | tf_op jit(solution)/shard_map/all_gather | solution.py:135
  13.1 13.5 %copy-start.14 = (f32[4]{0:T(128)S(1)}, f32[4]{0:T(128)}, u32[]{:S(2)}) copy-start(f32[4]{0:T(128)} %param.28) | copy-start | bytes 52
  20.7 2.8 copy-start.17
  23.4 154.4 %all-gather.15.cloned.1.call-start = ((), (), s32[]{:S(2)}) async-start(), calls=%async_computation.3 | async-start | bytes 4456448 | tf_op jit(solution)/shard_map/all_gather | solution.py:134
  26.5 343.5 %all-gather.23.cloned.1.call-start = ((), (), s32[]{:S(2)}) async-start(), calls=%async_computation.8 | async-start | bytes 17825792 | tf_op jit(solution)/shard_map/all_gather | solution.py:15
  35.7 2.2 copy-start.15
  35.7 2.5 copy-start.18
  38.2 51.4 %copy-start.7 = (f32[256,4,128]{2,0,1:T(8,128)}, f32[256,4,128]{2,0,1:T(8,128)S(1)}, u32[]{:S(2)}) copy-start(f32[256,4,128]{2,0,1:T(8,128)S(1)} %get-tuple-element.333) | copy-start | bytes 1572868
  38.2 51.4 %copy-start.9 = (f32[256,4,128]{2,0,1:T(8,128)}, f32[256,4,128]{2,0,1:T(8,128)S(1)}, u32[]{:S(2)}) copy-start(f32[256,4,128]{2,0,1:T(8,128)S(1)} %get-tuple-element.334) | copy-start | bytes 1572868
  38.2 6.9 %copy-start.20 = (u32[32]{0:T(128)S(1)}, u32[32]{0:T(128)}, u32[]{:S(2)}) copy-start(u32[32]{0:T(128)} %constant.118) | copy-start | bytes 388
  41.7 384.1 %all-gather.19.cloned.1.call-start = ((), (), s32[]{:S(2)}) async-start(), calls=%async_computation.5 | async-start | bytes 1114112 | tf_op jit(solution)/shard_map/all_gather | solution.py:144
  42.2 473.7 %all-gather.21.cloned.1.call-start = ((), (), s32[]{:S(2)}) async-start(), calls=%async_computation.6 | async-start | bytes 4456448 | tf_op jit(solution)/shard_map/all_gather | solution.py:194
  42.8 537.0 %all-gather.17.cloned.1.call-start = ((), (), s32[]{:S(2)}) async-start(), calls=%async_computation.4 | async-start | bytes 2228224 | tf_op jit(solution)/shard_map/all_gather | solution.py:193
  43.6 547.0 %reduce-scatter.2.cloned.1.call-start = ((), (), s32[]{:S(2)}) async-start(), calls=%async_computation.7 | async-start | bytes 1572864 | tf_op jit(solution)/shard_map/reduce_scatter | solution.py:197
  89.5 3.2 copy-start.16
  89.5 3.2 copy-start.19
  90.9 87.8 %copy-start.11 = (f32[4]{0:T(128)S(1)}, f32[4]{0:T(128)}, u32[]{:S(2)}) copy-start(f32[4]{0:T(128)} %param.27) | copy-start | bytes 52
  178.7 38.3 %copy-start.13 = (f32[512]{0:T(512)S(1)}, f32[512]{0:T(512)}, u32[]{:S(2)}) copy-start(f32[512]{0:T(512)} %param.30) | copy-start | bytes 6148
  198.2 2.1 copy-start.2
  203.0 2.2 copy-start.3
  205.2 6.6 %copy-start.4 = (f32[256,4,128]{0,2,1:T(8,128)S(1)}, f32[256,4,128]{0,2,1:T(8,128)}, u32[]{:S(2)}) copy-start(f32[256,4,128]{0,2,1:T(8,128)} %get-tuple-element.497) | copy-start | bytes 1572868 | tf_op jit(solution)/shard_map/while
  212.3 0.8 copy-start.5
  370.1 55.7 %copy-start.6 = (f32[256,4,256]{0,2,1:T(8,128)S(1)}, f32[256,4,256]{0,2,1:T(8,128)}, u32[]{:S(2)}) copy-start(f32[256,4,256]{0,2,1:T(8,128)} %convolution_bitcast_fusion.2) | copy-start | bytes 3145732
  370.1 55.7 %copy-start.8 = (f32[256,4,128]{2,0,1:T(8,128)S(1)}, f32[256,4,128]{2,0,1:T(8,128)}, u32[]{:S(2)}) copy-start(f32[256,4,128]{2,0,1:T(8,128)} %copy-done.7) | copy-start | bytes 1572868
  370.1 55.7 %copy-start.10 = (f32[256,4,128]{2,0,1:T(8,128)S(1)}, f32[256,4,128]{2,0,1:T(8,128)}, u32[]{:S(2)}) copy-start(f32[256,4,128]{2,0,1:T(8,128)} %copy-done.9) | copy-start | bytes 1572868
  425.8 3.8 copy-start.12
  516.0 74.6 %copy-start.1 = (bf16[2048,512]{1,0:T(8,128)(2,1)S(1)}, bf16[2048,512]{1,0:T(8,128)(2,1)}, u32[]{:S(2)}) copy-start(bf16[2048,512]{1,0:T(8,128)(2,1)} %param.23) | copy-start | bytes 6291460
Sparse Core Ops, SparseCore 0:
  8.9 11.7 all-gather.10
  23.5 77.1 all-gather.12
  103.5 74.2 all-gather.14
  180.4 189.5 all-gather.22
  372.7 53.0 all-gather.18
  428.3 87.5 all-gather.20
  518.7 61.1 all-gather.16
  583.9 6.5 reduce-scatter.1
where the time goes:
time: 599 us; the launch traced here: 597 us
  waiting for transfers between devices  412 us (69%)
  other arithmetic  66 us (11%)
  blocking collectives  50.3 us (8%)
  matrix products  39.7 us (7%)
  between operations  15 us (3%)
  local copies, waits for them, and re-layouts  14 us (2%)
    all_gather x1, waiting for transfers between devices, entering_2(): pieces = jax.tree.map(lambda part: lax.all_gather(part, axis), value)  152 us
    all_gather x1, waiting for transfers between devices, body(): lax.all_gather(ret_out_w, 'sp', axis=1, tiled=True)  86.2 us
    all_gather x1, waiting for transfers between devices, body(): lax.all_gather(stick_key, 'sp', axis=0, tiled=True)  77.1 us
    all_gather x1, waiting for transfers between devices, body(): lax.all_gather(stick_out_w, 'sp', axis=1, tiled=True)  58.9 us
    unnamed x1, blocking collectives  43.1 us
    select_n x15, other arithmetic, hop(): jnp.where(position < mine, new, old)  41.1 us
    dot_general x6, matrix products, body(): jnp.dot(scaled, matrix, preferred_element_type=jnp.float32)  15.1 us
    all_gather x1, waiting for transfers between devices, body(): state_full = lax.all_gather(initial_state, 'sp', axis=1, tiled=True)  14.5 us
  transfers between devices with their start and end apart: 8, of which 8 were waited for; matrix products, arithmetic and copies ran while one was open for 18% of the time, Pallas kernels for 0%

commit v1 on v0

--- a/solution.py
+++ b/solution.py
@@ -191,7 +191,7 @@
     ret_normed = (normed.reshape(tok_rows, ret_heads * ret_width) * ret_gain).astype(jnp.bfloat16)
     stick_cols, ret_cols = (
         lax.all_gather(stick_out_w, "sp", axis=1, tiled=True),
-        lax.all_gather(ret_out_w, "sp", axis=1, tiled=True),
+        jnp.concatenate(lax.all_gather(ret_out_w, "sp"), axis=1),
     )
     stick_part = jnp.dot(stick_normed, stick_cols, preferred_element_type=jnp.float32)
     return lax.psum_scatter(

time: 599 us -> 586 us (0.978)
  waiting for transfers between devices: 412 us -> 395 us
  local copies, waits for them, and re-layouts: 14 us -> 20.4 us
    all_gather x1, waiting for transfers between devices: 86.2 us -> 7.08 us  [body(): lax.all_gather(ret_out_w, 'sp')]
    all_gather x1, waiting for transfers between devices: 6.52 us -> 70.7 us  [body(): lax.all_gather(stick_value, 'sp', axis=0, tiled=True)]
    reshape x0 -> x1, local copies, waits for them, and re-layouts: none -> 6.39 us  [body(): jnp.concatenate(lax.all_gather(ret_out_w, 'sp'), axis=1)]
  transfers between devices with their start and end apart: 8 -> 8, of which waited for: 8 -> 8; matrix products, arithmetic and copies ran while one was open for 18% -> 20% of each run, Pallas kernels for 0% -> 0%
where the time goes in v1:
time: 586 us; the launch traced here: 585 us
  waiting for transfers between devices  395 us (67%)
  other arithmetic  65.9 us (11%)
  blocking collectives  50.3 us (9%)
  matrix products  37.5 us (6%)
  local copies, waits for them, and re-layouts  20.4 us (3%)
  between operations  15 us (3%)
    all_gather x1, waiting for transfers between devices, entering_2(): pieces = jax.tree.map(lambda part: lax.all_gather(part, axis), value)  152 us
    all_gather x1, waiting for transfers between devices, body(): lax.all_gather(stick_key, 'sp', axis=0, tiled=True)  76.8 us
    all_gather x1, waiting for transfers between devices, body(): lax.all_gather(stick_value, 'sp', axis=0, tiled=True)  70.7 us
    all_gather x1, waiting for transfers between devices, body(): lax.all_gather(stick_out_w, 'sp', axis=1, tiled=True)  57.8 us
    unnamed x1, blocking collectives  43 us
    select_n x15, other arithmetic, hop(): jnp.where(position < mine, new, old)  41.1 us
    dot_general x6, matrix products, body(): jnp.dot(scaled, matrix, preferred_element_type=jnp.float32)  15.1 us
    all_gather x1, waiting for transfers between devices, body(): state_full = lax.all_gather(initial_state, 'sp', axis=1, tiled=True)  14.5 us
  transfers between devices with their start and end apart: 8, of which 8 were waited for; matrix products, arithmetic and copies ran while one was open for 20% of the time, Pallas kernels for 0%

profile of v1, /device:TPU:0, one launch (start us, length us, event | category | flops | bytes accessed | tf_op | source)
XLA Modules:
  0.0 584.7 jit_solution(15316957618424131384)
XLA Ops:
  6.5 0.7 all-gather.12.cloned.1.call-update
  7.3 0.7 all-gather.24.cloned.1.call-update
  8.1 2.1 all-gather
  10.2 1.2 multiply_reduce_fusion.1
  11.4 2.5 psum.14
  13.9 6.8 %all-gather.12.cloned.1.call-done = bf16[256,2048]{1,0:T(8,128)(2,1)} async-done(((bf16[256,1024]{1,0:T(8,128)(2,1)}), bf16[256,2048]{1,0:T(8,128)(2,1)}) %all-gather.12.cloned.1.call-update) | async-done | bytes 1048592 | tf_op jit(solution)/shard_map/all_gather | solution.py:117
  20.7 2.7 fusion.29
  23.5 3.0 fusion.30
  27.3 3.4 fusion.26
  31.2 3.9 fusion.28
  36.4 1.5 copy-done.16
  38.2 1.3 fusion.24
  39.5 2.2 fusion.35
  42.3 0.7 all-gather.18.cloned.1.call-update
  43.2 0.6 slice.25
  44.4 0.6 dynamic-slice
  45.7 43.0 %all-reduce = f32[64]{0:T(128)S(1)} all-reduce(f32[64]{0:T(128)S(1)} %get-tuple-element.356), channel_id=3, replica_groups=mesh['sp'=16,'tp'=2] {'sp'}, use_global_device_ids=true, to_apply=%add | all-reduce | flops 64 | bytes 512
  88.9 1.3 convolution_multiply_fusion
  90.3 1.8 convolution_bitcast_fusion.2
  92.1 0.7 fusion.32
  92.8 0.8 copy.107
  93.5 7.1 %all-gather.24.cloned.1.call-done = bf16[16384,128]{1,0:T(8,128)(2,1)} async-done(((bf16[1024,128]{1,0:T(8,128)(2,1)}), bf16[16384,128]{1,0:T(8,128)(2,1)}) %all-gather.24.cloned.1.call-update) | async-done | bytes 4194320 | tf_op jit(solution)/shard_map/all_gather | solution.py:194
  100.6 6.4 %copy.75 = bf16[1024,16,128]{0,2,1:T(8,128)(2,1)} copy(bf16[1024,16,128]{2,0,1:T(8,128)(2,1)} %bitcast.123) | data formatting | bytes 8388608 | tf_op jit(solution)/shard_map/reshape | solution.py:194
  107.0 70.7 %all-gather.14.cloned.1.call-done = bf16[4096,512]{1,0:T(8,128)(2,1)} async-done(((bf16[256,512]{1,0:T(8,128)(2,1)}), bf16[4096,512]{1,0:T(8,128)(2,1)}) %all-gather.14.cloned.1.call-update) | async-done | bytes 4194320 | tf_op jit(solution)/shard_map/all_gather | solution.py:135
  177.7 76.8 %all-gather.16.cloned.1.call-done = bf16[4096,512]{1,0:T(8,128)(2,1)} async-done(((bf16[256,512]{1,0:T(8,128)(2,1)}), bf16[4096,512]{1,0:T(8,128)(2,1)}) %all-gather.16.cloned.1.call-update) | async-done | bytes 4194320 | tf_op jit(solution)/shard_map/all_gather | solution.py:134
  254.6 0.8 broadcast_in_dim.37
  255.5 34.5 %while.29 = (s32[]{:T(128)}, f32[256,4,128]{0,2,1:T(8,128)}, f32[4,256]{1,0:T(4,128)S(1)}, s32[]{:T(128)}, s32[]{:T(128)}, /*index=5*/bf16[4096,512]{1,0:T(8,128...) while((s32[]{:T(128)}, f32[256,4,128]{0,2,1:T(8,128)}, ...), condition=%wide.region_6.7_spmd.clone, body=%wide.region_2.6_spmd.clone.sunk | while | flops 707463424 | bytes 96735608 | solution.py:91
  255.5 1.7 constant_dynamic-slice_fusion.3
  257.1 0.5 copy.113
  258.1 0.5 copy.114
  258.6 6.3 %fusion.88 = (f32[4,256]{1,0:T(4,128)S(1)}, f32[4,256,1024]{1,2,0:T(8,128)S(1)}, f32[4,1024,256]{2,1,0:T(8,128)}) fusion(f32[4]{0:T(128)S(1)} %get-tuple-element.529, pred[256,1024]{0,1:T(8,128)(4,1)S(1)} %compare_and_fusion.2, bf16[1024,4,128]{0,2,1:T(8,128)(2,1)S(1)} %bitcast.122, bf16[256,4,128]{2,0,1:T(8,128)(2,1)} %get-tuple-element.528), kind=kOutput, calls=%fused_computation.33.clone.1 | convolution fusion | flops 279968768 | bytes 9965584 | tf_op jit(solution)/shard_map/while/body/thd,shd->hts/dot_general | solution.py:48
  264.9 10.1 %fusion.89 = f32[4,256,8,128]{1,2,3,0:T(8,128)S(1)} fusion(f32[4,256,8,128]{1,3,2,0:T(8,128)S(1)} %bitcast.120), kind=kOutput, calls=%fused_computation.20.clone.1 | output fusion | flops 133169152 | bytes 8388608 | tf_op jit(solution)/shard_map/reduce-window.4
  275.0 2.1 copy-done.2
  277.1 2.7 broadcast_add_fusion.2
  279.8 1.3 copy.115
  281.1 0.9 copy-done.3
  282.0 6.6 %fusion.90 = bf16[4,256,1024]{1,2,0:T(8,128)(2,1)S(1)} fusion(f32[4,256,8,128]{1,3,2,0:T(8,128)S(1)} %copy.115, f32[4,1024,256]{2,1,0:T(8,128)S(1)} %copy-done.3, f32[4,256]{1,0:T(4,128)S(1)} %get-tuple-element.508, f32[4]{0:T(128)S(1)} %get-tuple-element.529, pred[256,1024]{0,1:T(8,128)(4,1)S(1)} %compare_and_fusion.2), kind=kLoop, calls=%fused_computation.8.clone.1 | loop fusion | flops 24117248 | bytes 10752016 | tf_op jit(solution)/shard_map/while/body/convert_element_type | solution.py:55
  289.2 0.8 copy-done.5
  290.0 1.1 multiply_reduce_fusion.2
  291.1 2.7 psum.15
  293.8 1.2 fusion.41
  295.0 151.9 %all-gather.22.cloned.1.call-done = f32[64,256,256]{2,1,0:T(8,128)} async-done(((f32[4,256,256]{2,1,0:T(8,128)}), f32[64,256,256]{2,1,0:T(8,128)}) %all-gather.22.cloned.1.call-update) | async-done | bytes 16777232 | tf_op jit(solution)/shard_map/all_gather | solution.py:15
  446.9 41.2 %while.30 = (s32[]{:T(128)}, f32[4,256,256]{2,1,0:T(8,128)}, s32[]{:T(128)}, f32[16,4]{1,0:T(8,128)S(1)}, f32[16,4,256,256]{3,2,1,0:T(8,128)}, /*index=5*/s32[]{:T(128)}, s32[]{:T(128)}) while((s32[]{:T(128)}, f32[4,256,256]{2,1,0:T(8,128)}, s32[]{:T(128)}, f32[16,4]{1,0:T(8,128)S(1)}, f32[16,4,256,256]{3,2,1,0:T(8,128)}, ...), condition=%wide.region_10.11_spmd.clone, body=%wide.region_9.10_spmd.clone.sunk | while | flops 1048580 | bytes 3145889 | solution.py:24
  446.9 2.6 fusion.92
  449.5 2.7 fusion.92
  452.3 2.7 fusion.92
  455.0 2.8 fusion.92
  457.8 2.7 fusion.92
  460.5 2.7 fusion.92
  463.3 2.7 fusion.92
  466.0 2.7 fusion.92
  468.8 2.7 fusion.92
  471.5 2.8 fusion.92
  474.3 2.7 fusion.92
  477.1 2.7 fusion.92
  479.8 2.8 fusion.92
  482.6 2.7 fusion.92
  485.4 2.7 fusion.92
  488.1 14.5 %all-gather.20.cloned.1.call-done = f32[4,256,256]{2,1,0:T(8,128)} async-done(((f32[4,16,256]{2,1,0:T(8,128)}), f32[4,256,256]{2,1,0:T(8,128)}) %all-gather.20.cloned.1.call-update) | async-done | bytes 1048592 | tf_op jit(solution)/shard_map/all_gather | solution.py:144
  502.6 3.7 fusion.56
  506.7 2.6 fusion.57
  509.3 57.8 %all-gather.18.cloned.1.call-done = bf16[512,2048]{1,0:T(8,128)(2,1)} async-done(((bf16[512,128]{1,0:T(8,128)(2,1)}), bf16[512,2048]{1,0:T(8,128)(2,1)}) %all-gather.18.cloned.1.call-update) | async-done | bytes 2097168 | tf_op jit(solution)/shard_map/all_gather | solution.py:193
  567.1 3.9 fusion.21
  571.1 6.7 %reduce-scatter.2.cloned.1.call-done = bf16[128,2048]{1,0:T(8,128)(2,1)} async-done(((bf16[256,2048]{1,0:T(8,128)(2,1)}), bf16[128,2048]{1,0:T(8,128)(2,1)}) %reduce-scatter.2.cloned.1.call-update) | async-done | bytes 524304 | tf_op jit(solution)/shard_map/reduce_scatter | solution.py:197
  (101 shorter events, 5.3 us)
Async XLA Ops:
  6.5 14.1 %copy-start = (bf16[2048,512]{1,0:T(8,128)(2,1)S(1)}, bf16[2048,512]{1,0:T(8,128)(2,1)}, u32[]{:S(2)}) copy-start(bf16[2048,512]{1,0:T(8,128)(2,1)} %param.23) | copy-start | bytes 6291460
  6.5 14.1 %all-gather.12.cloned.1.call-start = ((), (), s32[]{:S(2)}) async-start(), calls=%async_computation.1 | async-start | bytes 1572864 | tf_op jit(solution)/shard_map/all_gather | solution.py:117
  7.3 93.4 %all-gather.24.cloned.1.call-start = ((), (), s32[]{:S(2)}) async-start(), calls=%async_computation.8 | async-start | bytes 4456448 | tf_op jit(solution)/shard_map/all_gather | solution.py:194
  8.0 169.7 %all-gather.14.cloned.1.call-start = ((), (), s32[]{:S(2)}) async-start(), calls=%async_computation.2 | async-start | bytes 4456448 | tf_op jit(solution)/shard_map/all_gather | solution.py:135
  13.9 12.7 %copy-start.15 = (f32[4]{0:T(128)S(1)}, f32[4]{0:T(128)}, u32[]{:S(2)}) copy-start(f32[4]{0:T(128)} %param.28) | copy-start | bytes 52
  20.7 2.8 copy-start.18
  23.4 231.2 %all-gather.16.cloned.1.call-start = ((), (), s32[]{:S(2)}) async-start(), calls=%async_computation.3 | async-start | bytes 4456448 | tf_op jit(solution)/shard_map/all_gather | solution.py:134
  26.5 420.4 %all-gather.22.cloned.1.call-start = ((), (), s32[]{:S(2)}) async-start(), calls=%async_computation.7 | async-start | bytes 17825792 | tf_op jit(solution)/shard_map/all_gather | solution.py:15
  35.7 2.2 copy-start.16
  35.7 2.5 copy-start.19
  38.2 50.7 %copy-start.8 = (f32[256,4,128]{2,0,1:T(8,128)}, f32[256,4,128]{2,0,1:T(8,128)S(1)}, u32[]{:S(2)}) copy-start(f32[256,4,128]{2,0,1:T(8,128)S(1)} %get-tuple-element.343) | copy-start | bytes 1572868
  38.2 50.8 %copy-start.10 = (f32[256,4,128]{2,0,1:T(8,128)}, f32[256,4,128]{2,0,1:T(8,128)S(1)}, u32[]{:S(2)}) copy-start(f32[256,4,128]{2,0,1:T(8,128)S(1)} %get-tuple-element.344) | copy-start | bytes 1572868
  38.2 6.2 %copy-start.21 = (u32[32]{0:T(128)S(1)}, u32[32]{0:T(128)}, u32[]{:S(2)}) copy-start(u32[32]{0:T(128)} %constant.118) | copy-start | bytes 388
  38.2 50.7 %copy-start.13 = (f32[1024]{0:T(1024)S(1)}, f32[1024]{0:T(1024)}, u32[]{:S(2)}) copy-start(f32[1024]{0:T(1024)} %param.31) | copy-start | bytes 12292
  41.7 460.9 %all-gather.20.cloned.1.call-start = ((), (), s32[]{:S(2)}) async-start(), calls=%async_computation.5 | async-start | bytes 1114112 | tf_op jit(solution)/shard_map/all_gather | solution.py:144
  42.2 524.9 %all-gather.18.cloned.1.call-start = ((), (), s32[]{:S(2)}) async-start(), calls=%async_computation.4 | async-start | bytes 2228224 | tf_op jit(solution)/shard_map/all_gather | solution.py:193
  43.0 534.8 %reduce-scatter.2.cloned.1.call-start = ((), (), s32[]{:S(2)}) async-start(), calls=%async_computation.6 | async-start | bytes 1572864 | tf_op jit(solution)/shard_map/reduce_scatter | solution.py:197
  88.9 3.2 copy-start.17
  88.9 3.2 copy-start.20
  100.6 154.8 %copy-start.12 = (f32[4]{0:T(128)S(1)}, f32[4]{0:T(128)}, u32[]{:S(2)}) copy-start(f32[4]{0:T(128)} %param.27) | copy-start | bytes 52
  255.5 38.3 %copy-start.14 = (f32[512]{0:T(512)S(1)}, f32[512]{0:T(512)}, u32[]{:S(2)}) copy-start(f32[512]{0:T(512)} %param.30) | copy-start | bytes 6148
  275.0 2.1 copy-start.2
  279.8 2.2 copy-start.3
  282.0 6.6 %copy-start.4 = (f32[256,4,128]{0,2,1:T(8,128)S(1)}, f32[256,4,128]{0,2,1:T(8,128)}, u32[]{:S(2)}) copy-start(f32[256,4,128]{0,2,1:T(8,128)} %get-tuple-element.507) | copy-start | bytes 1572868 | tf_op jit(solution)/shard_map/while
  289.1 0.8 copy-start.5
  446.9 55.7 %copy-start.7 = (f32[256,4,256]{0,2,1:T(8,128)S(1)}, f32[256,4,256]{0,2,1:T(8,128)}, u32[]{:S(2)}) copy-start(f32[256,4,256]{0,2,1:T(8,128)} %convolution_bitcast_fusion.2) | copy-start | bytes 3145732
  446.9 55.7 %copy-start.9 = (f32[256,4,128]{2,0,1:T(8,128)S(1)}, f32[256,4,128]{2,0,1:T(8,128)}, u32[]{:S(2)}) copy-start(f32[256,4,128]{2,0,1:T(8,128)} %copy-done.8) | copy-start | bytes 1572868
  446.9 55.7 %copy-start.11 = (f32[256,4,128]{2,0,1:T(8,128)S(1)}, f32[256,4,128]{2,0,1:T(8,128)}, u32[]{:S(2)}) copy-start(f32[256,4,128]{2,0,1:T(8,128)} %copy-done.10) | copy-start | bytes 1572868
  502.6 4.1 copy-start.6
  506.6 71.2 %copy-start.1 = (bf16[2048,512]{1,0:T(8,128)(2,1)S(1)}, bf16[2048,512]{1,0:T(8,128)(2,1)}, u32[]{:S(2)}) copy-start(bf16[2048,512]{1,0:T(8,128)(2,1)} %param.23) | copy-start | bytes 6291460
Sparse Core Ops, SparseCore 0:
  8.9 11.7 all-gather.11
  23.4 77.1 all-gather.23
  103.4 74.3 all-gather.13
  180.4 74.1 all-gather.15
  257.2 189.6 all-gather.21
  449.5 53.0 all-gather.19
  505.3 61.8 all-gather.17
  571.2 6.5 reduce-scatter.1
